TPU v7x, 32 devices: a whole 2x2x4 slice. The times are simulated.
32 devices in a mesh: sp: 8 (over z, y), tp: 4 (over x, core).
Axes of the slice: x: 2, y: 2, z: 4, core: 2. Of those that a mesh axis runs over, the one named last changes fastest.
Arguments:
- values_in: bfloat16 [4, 8192, 1024], P(None, 'sp', 'tp'), may hold values from -6 to 6
- gates_in: bfloat16 [4, 8192, 1024], P(None, 'sp', 'tp'), may hold values from -8 to 8
- conv_taps: bfloat16 [31, 1024], P(None, 'tp'), may hold values from -3 to 3
- conv_bias: bfloat16 [1024], P('tp'), may hold values from -3 to 3
- norm_gain: bfloat16 [1024], P('tp'), may hold values from 0.099609375 to 1.8984375
- out_weight: bfloat16 [1024, 4096], P('tp'), may hold values from -0.1875 to 0.1875
- out_grad: bfloat16 [4, 8192, 4096], P(None, 'sp'), may hold values from -1.5 to 1.5
Outputs:
- values_grad: bfloat16 [4, 8192, 1024], P(None, 'sp', 'tp')
- gates_grad: bfloat16 [4, 8192, 1024], P(None, 'sp', 'tp')
- taps_grad: float32 [31, 1024], P(None, 'tp')
- gain_grad: float32 [1024], P('tp')
- bias_grad: float32 [1024], P('tp')
- weight_grad: float32 [1024, 4096], P(('tp', 'sp'))
All inputs are finite; a program needn't handle non-finite values.
Results may differ from a plain program's by a relative error of at most 0.0048.
Values may be sent and summed in bfloat16 or wider, within the bound.
A program may use at most 128 MiB of HBM per device.

v0:
```python
import jax
import jax.numpy as jnp
from jax import lax
from jax.sharding import PartitionSpec as P

K = 31


EPS = 1e-05


def passed_along(shard, axis, by):
    devices = lax.axis_size(axis)
    pairs = [(i, i + by) for i in range(devices) if 0 <= i + by < devices]
    return lax.ppermute(shard, axis, pairs)


def on_device(values_in, gates_in, conv_taps, conv_bias, norm_gain, out_weight, out_grad):
    seq_count, tok_rows, local_chans = values_in.shape
    reach = K - 1
    total_chans = local_chans * lax.axis_size("tp")
    sig = jax.nn.sigmoid(gates_in.astype(jnp.float32))
    gated = (values_in.astype(jnp.float32) * sig).astype(jnp.bfloat16)
    before = passed_along(gated[:, tok_rows - reach :], "sp", 1)
    padded = jnp.concatenate([before, gated], axis=1).astype(jnp.float32)
    tap_rows = conv_taps.astype(jnp.float32)
    conv = jnp.zeros(gated.shape, jnp.float32) + conv_bias.astype(jnp.float32)
    for tap_index in range(K):
        conv = conv + tap_rows[tap_index] * padded[:, tap_index : tap_index + tok_rows]
    totals = lax.psum((jnp.sum(conv, axis=-1), jnp.sum(conv * conv, axis=-1)), "tp")
    channel_mean = totals[0][..., None] / total_chans
    variance = totals[1][..., None] / total_chans - channel_mean * channel_mean
    inverse = lax.rsqrt(variance + EPS)
    normed = (conv - channel_mean) * inverse
    gain = norm_gain.astype(jnp.float32)
    scaled = normed * gain
    swished = jax.nn.silu(scaled).astype(jnp.bfloat16)
    flat_swished = swished.reshape(seq_count * tok_rows, local_chans)
    flat_cot = out_grad.reshape(seq_count * tok_rows, out_grad.shape[2])
    weight_grad = lax.psum_scatter(
        lax.dot_general(
            flat_swished, flat_cot, (((0,), (0,)), ((), ())), preferred_element_type=jnp.float32
        ),
        "sp",
        scatter_dimension=0,
        tiled=True,
    )
    swish_grad = jnp.einsum("std,cd->stc", out_grad, out_weight, preferred_element_type=jnp.float32)
    scaled_sig = jax.nn.sigmoid(scaled)
    scaled_grad = swish_grad * scaled_sig * (1.0 + scaled * (1.0 - scaled_sig))
    gain_local = jnp.sum(scaled_grad * normed, axis=(0, 1))
    normed_grad = scaled_grad * gain
    back_sums = lax.psum(
        (jnp.sum(normed_grad, axis=-1), jnp.sum(normed_grad * normed, axis=-1)), "tp"
    )
    conv_grad = inverse * (
        normed_grad
        - back_sums[0][..., None] / total_chans
        - normed * (back_sums[1][..., None] / total_chans)
    )
    bias_local = jnp.sum(conv_grad, axis=(0, 1))
    taps_local = jnp.stack(
        [
            jnp.sum(conv_grad * padded[:, tap_index : tap_index + tok_rows], axis=(0, 1))
            for tap_index in range(K)
        ]
    )
    taps_grad, gain_grad, bias_grad = lax.psum((taps_local, gain_local, bias_local), "sp")
    wide_grad = jnp.pad(conv_grad, ((0, 0), (reach, reach), (0, 0)))
    spread = jnp.zeros((seq_count, tok_rows + reach, local_chans), jnp.float32)
    for tap_index in range(K):
        begin = reach - tap_index
        spread = spread + tap_rows[tap_index] * wide_grad[:, begin : begin + tok_rows + reach]
    arrived = passed_along(spread[:, :reach], "sp", -1)
    own = spread[:, reach:]
    gated_grad = jnp.concatenate(
        [own[:, : tok_rows - reach], own[:, tok_rows - reach :] + arrived], axis=1
    )
    values_grad = (gated_grad * sig).astype(jnp.bfloat16)
    gates_grad = (gated_grad * values_in.astype(jnp.float32) * sig * (1.0 - sig)).astype(
        jnp.bfloat16
    )
    return (values_grad, gates_grad, taps_grad, gain_grad, bias_grad, weight_grad)


def solution(mesh):
    return jax.shard_map(
        on_device,
        mesh=mesh,
        in_specs=(
            P(None, "sp", "tp"),
            P(None, "sp", "tp"),
            P(None, "tp"),
            P("tp"),
            P("tp"),
            P("tp", None),
            P(None, "sp", None),
        ),
        out_specs=(
            P(None, "sp", "tp"),
            P(None, "sp", "tp"),
            P(None, "tp"),
            P("tp"),
            P("tp"),
            P(("tp", "sp"), None),
        ),
        check_vma=False,
    )
```

profile of v0, /device:TPU:0, one launch (start us, length us, event | category | flops | bytes accessed | tf_op | source)
XLA Modules:
  0.0 227.2 jit_solution(9467286181582564596)
XLA Ops:
  7.2 0.0 copy-start
  7.2 0.0 reduce-scatter.2.cloned.1.call-start
  7.3 3.8 %fusion = bf16[4,1024,256]{2,1,0:T(8,128)(2,1)S(1)} fusion(bf16[4,1024,256]{2,1,0:T(8,128)(2,1)} %param.7, bf16[4,1024,256]{2,1,0:T(8,128)(2,1)} %param.8), kind=kLoop, calls=%fused_computation.4 | loop fusion | flops 7340032 | bytes 6291456 | tf_op jit(solution)/shard_map/convert_element_type | solution.py:23
  11.1 4.9 %collective-permute-start = (bf16[4,30,256]{2,1,0:T(8,128)(2,1)S(1)}, bf16[4,30,256]{2,1,0:T(8,128)(2,1)S(1)}, u32[]{:S(2)}, u32[]{:S(2)}) collective-permute-start(bf16[4,30,256]{2,1,0:T(8,128)(2,1)S(1)} %slice.454), channel_id=1, source_target_pairs={{0,4},{4,8},{8,12},{12,16},{16,20},{20,24},{24,28},{1,5},{5,9},{9,... | collective-permute-start | bytes 184328 | tf_op jit(solution)/shard_map/ppermute | solution.py:15
  16.1 1.8 collective-permute-done
  17.9 0.4 maximum_convert_fusion
  18.3 19.4 %multiply_reduce_fusion.33 = (f32[4,1024]{1,0:T(4,128)S(1)}, f32[4,1024]{1,0:T(4,128)S(1)}, f32[4,1024,256]{2,1,0:T(8,128)}) fusion(f32[4,1054,256]{2,1,0:T(8,128)S(1)} %maximum_convert_fusion, f32[256]{0:T(256)S(1)} %bitcast.133, f32[256]{0:T(256)S(1)} %bitcast.131, f32[256]{0:T(256)S(1)} %bitcast.129, f32[256]{0:T(256)S(1)} %bitcast.127, ...), kind=kLoop, calls=%fused_computation.48 | loop fusion | flops 68149248 | bytes 134283264 | tf_op jit(solution)/shard_map/reduce_sum | solution.py:30
  37.7 10.5 %all-reduce.3 = (f32[4,1024]{1,0:T(4,128)S(1)}, f32[4,1024]{1,0:T(4,128)S(1)}) all-reduce(f32[4,1024]{1,0:T(4,128)S(1)} %get-tuple-element.42, f32[4,1024]{1,0:T(4,128)S(1)} %get-tuple-element.41), channel_id=1, replica_groups=mesh['sp'=8,'tp'=4] {'tp'}, use_global_device_ids=true, to_apply=%region_3.0 | all-reduce | flops 8192 | bytes 65536 | tf_op jit(solution)/shard_map/psum | solution.py:30
  48.2 23.3 %convolution_bitcast_fusion = f32[256,4096]{1,0:T(8,128)} fusion(bf16[4,1024,4096]{2,1,0:T(8,128)(2,1)} %param.13, f32[4,1024,256]{2,1,0:T(8,128)} %get-tuple-element.51, f32[256]{0:T(256)S(1)} %convert_element_type.39, f32[4,1024]{1,0:T(4,128)S(1)} %get-tuple-element.55, f32[4,1024]{1,0:T(4,128)S(1)} %get-tuple-element.54), kind=kOutput, calls=%fused_computation | convolution fusion | flops 8598323200 | bytes 41976832 | tf_op jit(solution)/shard_map/dot_general | solution.py:41
  71.5 0.0 reduce-scatter.2.cloned.1.call-update
  71.6 19.8 %multiply_reduce_fusion = (f32[256]{0:T(256)S(1)}, f32[4,1024]{1,0:T(4,128)S(1)}, f32[4,1024]{1,0:T(4,128)S(1)}, f32[4,1024,256]{2,1,0:T(8,128)}) fusion(f32[4,1024,256]{2,1,0:T(8,128)} %get-tuple-element.51, f32[4,1024]{1,0:T(4,128)S(1)} %get-tuple-element.55, f32[4,1024]{1,0:T(4,128)S(1)} %get-tuple-element.54, f32[256]{0:T(256)S(1)} %convert_element_type.39, ...), kind=kOutput, calls=%fused_computation.10 | convolution fusion | flops 8607752192 | bytes 44107776 | tf_op jit(solution)/shard_map/std,cd->stc/dot_general | solution.py:48
  91.4 11.6 %all-reduce.2 = (f32[4,1024]{1,0:T(4,128)S(1)}, f32[4,1024]{1,0:T(4,128)S(1)}) all-reduce(f32[4,1024]{1,0:T(4,128)S(1)} %get-tuple-element.38, f32[4,1024]{1,0:T(4,128)S(1)} %get-tuple-element.39), channel_id=1, replica_groups=mesh['sp'=8,'tp'=4] {'tp'}, use_global_device_ids=true, to_apply=%region_7.8 | all-reduce | flops 8192 | bytes 65536 | tf_op jit(solution)/shard_map/psum | solution.py:53
  103.0 42.2 %multiply_reduce_fusion.1 = (f32[256]{0:T(256)S(1)}, f32[256]{0:T(256)S(1)}, f32[256]{0:T(256)S(1)}, f32[256]{0:T(256)S(1)}, f32[256]{0:T(256)S(1)}, /*index=5*/...) fusion(f32[4,1054,256]{2,1,0:T(8,128)} %copy-done.2, ...), kind=kLoop, calls=%fused_computation.11 | loop fusion | flops 45084160 | bytes 88165376 | tf_op jit(solution)/shard_map/reduce_sum | solution.py:64
  145.2 0.0 slice-start
  145.2 0.0 slice-start.1
  145.2 16.2 %multiply_add_fusion = f32[4,1054,256]{2,1,0:T(8,128)S(1)} fusion(f32[4,1024,256]{2,1,0:T(8,128)S(1)} %get-tuple-element.50, f32[256]{0:T(256)S(1)} %bitcast.134, f32[256]{0:T(256)S(1)} %bitcast.132, f32[256]{0:T(256)S(1)} %bitcast.130, f32[256]{0:T(256)S(1)} %bitcast.128, f32[256]{0:T(256)S(1)} %bitcast.126, f32[256]{0:T(256)S(1)} %bitcast.124, ...), kind=kLoop, calls=%fused_computation.3 | loop fusion | flops 65837056 | bytes 8543232 | tf_op jit(solution)/shard_map/add | solution.py:73
  161.4 1.3 collective-permute-start.1
  162.8 7.3 %multiply_reduce_fusion.19 = (f32[256]{0:T(256)S(1)}, f32[256]{0:T(256)S(1)}, f32[256]{0:T(256)S(1)}, f32[256]{0:T(256)S(1)}, f32[256]{0:T(256)S(1)}, /*index=5*...) fusion(f32[4,1024,256]{2,1,0:T(8,128)S(1)} %get-tuple-element.5, ...), kind=kLoop, calls=%fused_computation.29 | loop fusion | flops 28307968 | bytes 58734592 | tf_op jit(solution)/shard_map/reduce_sum | solution.py:64
  170.1 2.2 slice.516
  172.3 0.1 stack.127
  172.4 41.2 %all-reduce.1 = (f32[31,256]{1,0:T(8,128)}, f32[256]{0:T(256)}, f32[256]{0:T(256)}) all-reduce(f32[31,256]{1,0:T(8,128)S(1)} %stack.127, f32[256]{0:T(256)S(1)} %get-tuple-element.37, f32[256]{0:T(256)S(1)} %get-tuple-element.40), channel_id=1, replica_groups=mesh['sp'=8,'tp'=4] {'sp'}, use_global_device_ids=true, to_apply=%region_39.40 | all-reduce | flops 8448 | bytes 67584 | tf_op jit(solution)/shard_map/psum | solution.py:68
  213.6 0.0 collective-permute-done.1
  213.6 1.1 slice_add_fusion
  214.7 5.6 %fusion.3 = (bf16[4,1024,256]{2,1,0:T(8,128)(2,1)}, bf16[4,1024,256]{2,1,0:T(8,128)(2,1)}) fusion(bf16[4,1024,256]{2,1,0:T(8,128)(2,1)} %param.7, f32[4,30,256]{2,1,0:T(8,128)S(1)} %slice_add_fusion, f32[4,994,256]{2,1,0:T(8,128)} %slice.516, bf16[4,1024,256]{2,1,0:T(8,128)(2,1)} %param.8), kind=kLoop, calls=%fused_computation.7 | loop fusion | flops 13631488 | bytes 12582912 | tf_op jit(solution)/shard_map/convert_element_type | solution.py:80
  (25 shorter events, 0.1 us)
Async XLA Ops:
  7.2 64.4 %copy-start = (bf16[256,4096]{1,0:T(8,128)(2,1)S(1)}, bf16[256,4096]{1,0:T(8,128)(2,1)}, u32[]{:S(2)}) copy-start(bf16[256,4096]{1,0:T(8,128)(2,1)} %param.12) | copy-start | bytes 6291460
  7.2 8.8 %copy-start.4 = (bf16[31,256]{1,0:T(8,128)(2,1)S(1)}, bf16[31,256]{1,0:T(8,128)(2,1)}, u32[]{:S(2)}) copy-start(bf16[31,256]{1,0:T(8,128)(2,1)} %param.9) | copy-start | bytes 47620
  7.2 8.9 %copy-start.5 = (bf16[256]{0:T(256)(128)(2,1)S(1)}, bf16[256]{0:T(256)(128)(2,1)}, u32[]{:S(2)}) copy-start(bf16[256]{0:T(256)(128)(2,1)} %param.11) | copy-start | bytes 1540
  7.2 8.9 %copy-start.6 = (bf16[256]{0:T(256)(128)(2,1)S(1)}, bf16[256]{0:T(256)(128)(2,1)}, u32[]{:S(2)}) copy-start(bf16[256]{0:T(256)(128)(2,1)} %param.10) | copy-start | bytes 1540
  7.2 213.1 %reduce-scatter.2.cloned.1.call-start = ((), (), s32[]{:S(2)}) async-start(), calls=%async_computation.1 | async-start | bytes 4718592 | tf_op jit(solution)/shard_map/reduce_scatter | solution.py:40
  11.1 6.8 %collective-permute-start = (bf16[4,30,256]{2,1,0:T(8,128)(2,1)S(1)}, bf16[4,30,256]{2,1,0:T(8,128)(2,1)S(1)}, u32[]{:S(2)}, u32[]{:S(2)}) collective-permute-start(bf16[4,30,256]{2,1,0:T(8,128)(2,1)S(1)} %slice.454), channel_id=1, source_target_pairs={{0,4},{4,8},{8,12},{12,16},{16,20},{20,24},{24,28},{1,5},{5,9},{9,... | collective-permute-start | bytes 184328 | tf_op jit(solution)/shard_map/ppermute | solution.py:15
  18.3 19.4 %copy-start.2 = (f32[4,1054,256]{2,1,0:T(8,128)}, f32[4,1054,256]{2,1,0:T(8,128)S(1)}, u32[]{:S(2)}) copy-start(f32[4,1054,256]{2,1,0:T(8,128)S(1)} %maximum_convert_fusion) | copy-start | bytes 12951556
  145.2 17.6 %slice-start = ((s8[4325376]{0:T(1024)(128)(4,1)}), s8[4194304]{0:T(1024)(128)(4,1)S(1)}, s32[]{:S(2)}) async-start(s8[4325376]{0:T(1024)(128)(4,1)} %bitcast.71), calls=%async_computation.2 | async-start | bytes 8388608
  145.2 17.6 %slice-start.1 = ((s8[4325376]{0:T(1024)(128)(4,1)}), s8[131072]{0:T(1024)(128)(4,1)S(1)}, s32[]{:S(2)}) async-start(s8[4325376]{0:T(1024)(128)(4,1)} %bitcast.71), calls=%async_computation.3 | async-start | bytes 262144
  161.4 8.6 %copy-start.3 = (f32[4,1054,256]{2,1,0:T(8,128)}, f32[4,1054,256]{2,1,0:T(8,128)S(1)}, u32[]{:S(2)}) copy-start(f32[4,1054,256]{2,1,0:T(8,128)S(1)} %multiply_add_fusion) | copy-start | bytes 12951556
  161.4 52.2 %collective-permute-start.1 = (f32[4,30,256]{2,1,0:T(8,128)S(1)}, f32[4,30,256]{2,1,0:T(8,128)S(1)}, u32[]{:S(2)}, u32[]{:S(2)}) collective-permute-start(f32[4,30,256]{2,1,0:T(8,128)S(1)} %slice.518), channel_id=1, source_target_pairs={{4,0},{8,4},{12,8},{16,12},{20,16},{24,20},{28,24},{5,1},{9,5},{13... | collective-permute-start | bytes 368648 | tf_op jit(solution)/shard_map/ppermute | solution.py:15
  213.6 6.7 %copy-start.1 = (bf16[256,4096]{1,0:T(8,128)(2,1)S(1)}, bf16[256,4096]{1,0:T(8,128)(2,1)}, u32[]{:S(2)}) copy-start(bf16[256,4096]{1,0:T(8,128)(2,1)} %param.12) | copy-start | bytes 6291460
Sparse Core Ops, SparseCore 0:
  71.7 90.3 reduce-scatter.1
where the time goes:
time: 227 us
  other arithmetic  96 us (42%)
  blocking collectives  63.3 us (28%)
  matrix products  43.1 us (19%)
  between operations  14.3 us (6%)
  starting transfers between devices  6.23 us (3%)
  local copies, waits for them, and re-layouts  2.41 us (1%)
    reduce_sum x2, other arithmetic, on_device(): jnp.sum(conv_grad * padded[:, tap_index:tap_index + tok_rows], axis=(0, 1))  49.5 us
    psum x1, blocking collectives, on_device(): lax.psum((taps_local, gain_local, bias_local), 'sp')  41.2 us
    dot_general x1, matrix products, on_device(): lax.dot_general(flat_swished, flat_cot, (((0,), (0,)), ((), ())), preferr...  23.3 us
    dot_general x1, matrix products, on_device(): jnp.einsum('std,cd->stc', out_grad, out_weight, preferred_element_type=jn...  19.8 us
    reduce_sum x1, other arithmetic, on_device(): jnp.sum(conv * conv, axis=-1)  19.4 us
    add x1, other arithmetic, on_device(): spread + tap_rows[tap_index] * wide_grad[:, begin:begin + tok_rows + reach]  16.2 us
    psum x1, blocking collectives, on_device(): lax.psum((jnp.sum(normed_grad, axis=-1), jnp.sum(normed_grad * normed, ax...  11.6 us
    psum x1, blocking collectives, on_device(): lax.psum((jnp.sum(conv, axis=-1), jnp.sum(conv * conv, axis=-1)), 'tp')  10.5 us
  transfers between devices with their start and end apart: 3, of which 1 were waited for; matrix products, arithmetic and copies ran while one was open for 42% of the time, Pallas kernels for 0%

commit v1 on v0

v1 whole, which is shorter than its diff:
```python
import functools

import jax
import jax.numpy as jnp
from jax import lax
from jax.experimental import pallas as pl
from jax.experimental.pallas import tpu as pltpu
from jax.sharding import PartitionSpec as P

K = 31
EPS = 1e-05
HALO = 32
LANES = 128
F32 = jnp.float32
BF16 = jnp.bfloat16
VMEM_LIMIT = 60 * 1024 * 1024


def sigmoid(x):
    return 0.5 * jnp.tanh(0.5 * x) + 0.5


def passed_along(shard, axis, by):
    devices = lax.axis_size(axis)
    pairs = [(i, i + by) for i in range(devices) if 0 <= i + by < devices]
    return lax.ppermute(shard, axis, pairs)


def fir(x_ref, w_ref, lane_block, start, taps, blocks, init):
    accs = [init] * blocks
    weights = [w_ref[lane_block, k] for k in taps]
    for offset in range(K + 8 * (blocks - 1)):
        piece = x_ref[lane_block, pl.ds(start + offset, 8), :]
        for a in range(blocks):
            k = offset - 8 * a
            if 0 <= k < K:
                term = weights[k] * piece
                accs[a] = term if accs[a] is None else accs[a] + term
    return accs


def lane_sums(x):
    return jnp.sum(x.T, axis=0, keepdims=True)


def row_spread(row):
    return jnp.broadcast_to(row, (LANES, LANES)).T


def forward_kernel(
    seq_blocks, values_ref, gates_ref, halo_ref, taps_ref, bias_ref, cot_ref, weight_ref,
    conv_ref, grad_ref, sums_ref, padded,
):
    step = pl.program_id(0)
    rows, chans = values_ref.shape
    lane_blocks = chans // LANES
    chunks = rows // LANES
    depth = cot_ref.shape[1] // chunks
    grad_ref[...] = jnp.zeros_like(grad_ref)

    @pl.when(step % seq_blocks == 0)
    def _():
        for h in range(lane_blocks):
            padded[h, :HALO, :] = halo_ref[0, :, h * LANES : (h + 1) * LANES].astype(F32)

    @pl.when(step % seq_blocks != 0)
    def _():
        for h in range(lane_blocks):
            padded[h, :HALO, :] = padded[h, rows:, :]

    def chunk(i, carry):
        first = pl.multiple_of(i * LANES, LANES)
        here = pl.ds(first, LANES)
        columns = pl.ds(pl.multiple_of(i * depth, depth), depth)
        grad_ref[...] += lax.dot_general(
            cot_ref[:, columns], weight_ref[:, columns], (((1,), (1,)), ((), ())),
            preferred_element_type=F32,
        )
        total = None
        for h in range(lane_blocks):
            lanes = slice(h * LANES, (h + 1) * LANES)
            sig = sigmoid(gates_ref[here, lanes].astype(F32))
            gated = (values_ref[here, lanes].astype(F32) * sig).astype(BF16).astype(F32)
            padded[h, pl.ds(first + HALO, LANES), :] = gated
            for c in range(LANES // 32):
                start = first + c * 32
                accs = fir(padded, taps_ref, h, start + HALO - K + 1, range(K), 4, bias_ref[h])
                for a in range(4):
                    conv_ref[pl.ds(pl.multiple_of(start + 8 * a, 8), 8), lanes] = accs[a]
        total = square = None
        for h in range(lane_blocks):
            conv = conv_ref[here, h * LANES : (h + 1) * LANES]
            total = conv if total is None else total + conv
            square = conv * conv if square is None else square + conv * conv
        row = step * chunks + i
        sums_ref[0, pl.ds(row, 1), :] = lane_sums(total)
        sums_ref[1, pl.ds(row, 1), :] = lane_sums(square)
        return carry

    lax.fori_loop(0, chunks, chunk, 0)


def middle_kernel(
    blocks, total_chans, conv_ref, grad_ref, stats_ref, gain_ref, cot_ref,
    normed_grad_ref, sums_ref, gain_grad_ref, weight_grad_ref, swished,
):
    step = pl.program_id(0)
    rows, chans = conv_ref.shape
    lane_blocks = chans // LANES
    chunks = rows // LANES
    width = cot_ref.shape[1] // chunks
    now = lax.rem(step, 2)
    before = 1 - now

    @pl.when(step == 0)
    def _():
        weight_grad_ref[...] = jnp.zeros_like(weight_grad_ref)
        gain_grad_ref[...] = jnp.zeros_like(gain_grad_ref)
        swished[1] = jnp.zeros(swished.shape[1:], BF16)

    fresh = jnp.where(step < blocks, 1.0, 0.0).astype(F32)
    block = jnp.minimum(step, blocks - 1)

    def chunk(i, carry):
        first = pl.multiple_of(i * LANES, LANES)
        here = pl.ds(first, LANES)
        columns = pl.ds(pl.multiple_of(i * width, width), width)
        weight_grad_ref[:, columns] += jnp.dot(
            swished[before], cot_ref[:, columns], preferred_element_type=F32
        )
        row = block * chunks + i
        mean = stats_ref[0, pl.ds(row, 1), :] / total_chans
        variance = stats_ref[1, pl.ds(row, 1), :] / total_chans - mean * mean
        inverse = row_spread(lax.rsqrt(variance + EPS))
        mean = row_spread(mean)
        plain = weighted = None
        for h in range(lane_blocks):
            lanes = slice(h * LANES, (h + 1) * LANES)
            gain = gain_ref[:, lanes]
            normed = (conv_ref[here, lanes] - mean) * inverse
            scaled = normed * gain
            sig = sigmoid(scaled)
            silu = scaled * sig
            swished[now, lanes, here] = silu.T.astype(BF16)
            scaled_grad = grad_ref[here, lanes] * (sig + silu * (1.0 - sig))
            normed_grad = scaled_grad * gain
            normed_grad_ref[here, lanes] = normed_grad
            product = scaled_grad * normed
            gain_grad_ref[:, lanes] += fresh * jnp.sum(
                product.reshape(LANES // 8, 8, LANES), axis=0
            )
            product = product * gain
            plain = normed_grad if plain is None else plain + normed_grad
            weighted = product if weighted is None else weighted + product
        sums_ref[0, pl.ds(row, 1), :] = lane_sums(plain)
        sums_ref[1, pl.ds(row, 1), :] = lane_sums(weighted)
        return carry

    lax.fori_loop(0, chunks, chunk, 0)


def backward_kernel(
    total_chans, values_ref, gates_ref, halo_ref, next_ref, taps_ref, conv_ref, normed_grad_ref,
    stats_ref, back_ref, gain_grad_ref,
    values_grad_ref, gates_grad_ref, small_ref, padded, wide, taps_acc, bias_acc,
):
    step = pl.program_id(0)
    rows, chans = values_ref.shape
    lane_blocks = chans // LANES
    chunks = rows // LANES

    @pl.when(step == 0)
    def _():
        taps_acc[...] = jnp.zeros_like(taps_acc)
        bias_acc[...] = jnp.zeros_like(bias_acc)

    for h in range(lane_blocks):
        lanes = slice(h * LANES, (h + 1) * LANES)
        padded[h, :HALO, :] = halo_ref[0, :, lanes].astype(F32)
        wide[h, rows:, :] = next_ref[0, :, lanes]

    def prepare(i, carry):
        first = pl.multiple_of(i * LANES, LANES)
        here = pl.ds(first, LANES)
        row = step * chunks + i
        mean = stats_ref[0, pl.ds(row, 1), :] / total_chans
        variance = stats_ref[1, pl.ds(row, 1), :] / total_chans - mean * mean
        inverse = row_spread(lax.rsqrt(variance + EPS))
        mean = row_spread(mean)
        plain = row_spread(back_ref[0, pl.ds(row, 1), :] / total_chans)
        weighted = row_spread(back_ref[1, pl.ds(row, 1), :] / total_chans)
        for h in range(lane_blocks):
            lanes = slice(h * LANES, (h + 1) * LANES)
            sig = sigmoid(gates_ref[here, lanes].astype(F32))
            gated = (values_ref[here, lanes].astype(F32) * sig).astype(BF16).astype(F32)
            padded[h, pl.ds(first + HALO, LANES), :] = gated
            normed = (conv_ref[here, lanes] - mean) * inverse
            conv_grad = inverse * (normed_grad_ref[here, lanes] - plain - normed * weighted)
            wide[h, here, :] = conv_grad
            bias_acc[h] += jnp.sum(conv_grad.reshape(LANES // 8, 8, LANES), axis=0)
        return carry

    lax.fori_loop(0, chunks, prepare, 0)

    for h in range(lane_blocks):

        def correlate(i, accs):
            start = pl.multiple_of(i * 32, 32)
            accs = list(accs)
            grads = [wide[h, pl.ds(pl.multiple_of(start + 8 * a, 8), 8), :] for a in range(4)]
            for offset in range(K + 24):
                piece = padded[h, pl.ds(start + HALO - K + 1 + offset, 8), :]
                for a in range(4):
                    k = offset - 8 * a
                    if 0 <= k < K:
                        accs[k] = accs[k] + grads[a] * piece
            return tuple(accs)

        accs = lax.fori_loop(
            0, rows // 32, correlate, tuple(taps_acc[h, k] for k in range(K))
        )
        for k in range(K):
            taps_acc[h, k] = accs[k]

    def spread(i, carry):
        start = pl.multiple_of(i * 32, 32)
        here = pl.ds(start, 32)
        for h in range(lane_blocks):
            lanes = slice(h * LANES, (h + 1) * LANES)
            accs = fir(wide, taps_ref, h, start, range(K - 1, -1, -1), 4, None)
            gated_grad = jnp.concatenate(accs, axis=0)
            sig = sigmoid(gates_ref[here, lanes].astype(F32))
            values_part = gated_grad * sig
            values_grad_ref[here, lanes] = values_part.astype(BF16)
            gates_grad_ref[here, lanes] = (
                values_part * values_ref[here, lanes].astype(F32) * (1.0 - sig)
            ).astype(BF16)
        return carry

    lax.fori_loop(0, rows // 32, spread, 0)

    @pl.when(step == pl.num_programs(0) - 1)
    def _():
        for h in range(lane_blocks):
            lanes = slice(h * LANES, (h + 1) * LANES)
            for k in range(K):
                small_ref[k : k + 1, lanes] = jnp.sum(taps_acc[h, k], axis=0, keepdims=True)
            small_ref[K : K + 1, lanes] = jnp.sum(bias_acc[h], axis=0, keepdims=True)
            small_ref[K + 1 : K + 2, lanes] = jnp.sum(
                gain_grad_ref[:, lanes], axis=0, keepdims=True
            )
            small_ref[K + 2 :, lanes] = jnp.zeros((small_ref.shape[0] - K - 2, LANES), F32)


def whole(shape):
    return pl.BlockSpec(shape, lambda i: (0,) * len(shape))


def on_device(values_in, gates_in, conv_taps, conv_bias, norm_gain, out_weight, out_grad):
    seqs, tokens, chans = values_in.shape
    width = out_grad.shape[2]
    total_chans = chans * lax.axis_size("tp")
    lane_blocks = chans // LANES
    positions = seqs * tokens
    rows = min(512, tokens)
    blocks = positions // rows
    stat_rows = positions // LANES

    values = values_in.reshape(positions, chans)
    gates = gates_in.reshape(positions, chans)
    cot = out_grad.reshape(positions, width)

    tail_sig = jax.nn.sigmoid(gates_in[:, tokens - HALO :].astype(F32))
    tail = (values_in[:, tokens - HALO :].astype(F32) * tail_sig).astype(BF16)
    before = passed_along(tail, "sp", 1)

    def by_lanes(rows_of):
        count = rows_of.shape[0]
        split = rows_of.astype(F32).reshape(count, lane_blocks, 1, LANES).transpose(1, 0, 2, 3)
        return jnp.broadcast_to(split, (lane_blocks, count, 8, LANES))

    taps8 = by_lanes(conv_taps)
    bias8 = by_lanes(conv_bias[None])[:, 0]
    gain = norm_gain.astype(F32)[None]

    params = pltpu.CompilerParams(
        dimension_semantics=("arbitrary",), vmem_limit_bytes=VMEM_LIMIT
    )
    tile = pl.BlockSpec((rows, chans), lambda i: (i, 0))
    seq_blocks = tokens // rows
    conv, swish_grad, sums = pl.pallas_call(
        functools.partial(forward_kernel, seq_blocks),
        grid=(blocks,),
        in_specs=[
            tile,
            tile,
            pl.BlockSpec((1, HALO, chans), lambda i: (i // seq_blocks, 0, 0)),
            whole(taps8.shape),
            whole(bias8.shape),
            pl.BlockSpec((rows, width), lambda i: (i, 0)),
            whole(out_weight.shape),
        ],
        out_specs=[tile, tile, whole((2, stat_rows, LANES))],
        out_shape=[
            jax.ShapeDtypeStruct((positions, chans), F32),
            jax.ShapeDtypeStruct((positions, chans), F32),
            jax.ShapeDtypeStruct((2, stat_rows, LANES), F32),
        ],
        scratch_shapes=[pltpu.VMEM((lane_blocks, rows + HALO, LANES), F32)],
        compiler_params=params,
        name="forward",
    )(values, gates, before, taps8, bias8, cot, out_weight)
    stats = lax.psum(sums, "tp")

    ahead = pl.BlockSpec((rows, chans), lambda i: (jnp.minimum(i, blocks - 1), 0))
    normed_grad, back, gain_local, weight_local = pl.pallas_call(
        functools.partial(middle_kernel, blocks, total_chans),
        grid=(blocks + 1,),
        in_specs=[
            ahead,
            ahead,
            whole((2, stat_rows, LANES)),
            whole((1, chans)),
            pl.BlockSpec((rows, width), lambda i: (jnp.maximum(i - 1, 0), 0)),
        ],
        out_specs=[
            ahead,
            whole((2, stat_rows, LANES)),
            whole((8, chans)),
            whole((chans, width)),
        ],
        out_shape=[
            jax.ShapeDtypeStruct((positions, chans), F32),
            jax.ShapeDtypeStruct((2, stat_rows, LANES), F32),
            jax.ShapeDtypeStruct((8, chans), F32),
            jax.ShapeDtypeStruct((chans, width), F32),
        ],
        scratch_shapes=[pltpu.VMEM((2, chans, rows), BF16)],
        compiler_params=params,
        name="middle",
    )(conv, swish_grad, stats, gain, cot)
    back = lax.psum(back, "tp")
    weight_grad = lax.psum_scatter(weight_local, "sp", scatter_dimension=0, tiled=True)

    def first_rows(x):
        return x.reshape(seqs, tokens, -1)[:, :HALO]

    def of_rows(x):
        return x.reshape(seqs, tokens, 1)[:, :HALO] / total_chans

    mean = of_rows(stats[0])
    inverse = lax.rsqrt(of_rows(stats[1]) - mean * mean + EPS)
    head = inverse * (
        first_rows(normed_grad)
        - of_rows(back[0])
        - (first_rows(conv) - mean) * inverse * of_rows(back[1])
    )
    after = passed_along(head, "sp", -1)

    seq_tile = pl.BlockSpec((tokens, chans), lambda i: (i, 0))
    halo_tile = pl.BlockSpec((1, HALO, chans), lambda i: (i, 0, 0))
    small_rows = -(-(K + 2) // 8) * 8
    values_grad, gates_grad, small = pl.pallas_call(
        functools.partial(backward_kernel, total_chans),
        grid=(seqs,),
        in_specs=[
            seq_tile,
            seq_tile,
            halo_tile,
            halo_tile,
            whole(taps8.shape),
            seq_tile,
            seq_tile,
            whole((2, stat_rows, LANES)),
            whole((2, stat_rows, LANES)),
            whole((8, chans)),
        ],
        out_specs=[seq_tile, seq_tile, whole((small_rows, chans))],
        out_shape=[
            jax.ShapeDtypeStruct((positions, chans), BF16),
            jax.ShapeDtypeStruct((positions, chans), BF16),
            jax.ShapeDtypeStruct((small_rows, chans), F32),
        ],
        scratch_shapes=[
            pltpu.VMEM((lane_blocks, tokens + HALO, LANES), F32),
            pltpu.VMEM((lane_blocks, tokens + HALO, LANES), F32),
            pltpu.VMEM((lane_blocks, K, 8, LANES), F32),
            pltpu.VMEM((lane_blocks, 8, LANES), F32),
        ],
        compiler_params=params,
        name="backward",
    )(values, gates, before, after, taps8, conv, normed_grad, stats, back, gain_local)
    small = lax.psum(small, "sp")
    return (
        values_grad.reshape(values_in.shape),
        gates_grad.reshape(values_in.shape),
        small[:K],
        small[K + 1],
        small[K],
        weight_grad,
    )


def solution(mesh):
    return jax.shard_map(
        on_device,
        mesh=mesh,
        in_specs=(
            P(None, "sp", "tp"),
            P(None, "sp", "tp"),
            P(None, "tp"),
            P("tp"),
            P("tp"),
            P("tp", None),
            P(None, "sp", None),
        ),
        out_specs=(
            P(None, "sp", "tp"),
            P(None, "sp", "tp"),
            P(None, "tp"),
            P("tp"),
            P("tp"),
            P(("tp", "sp"), None),
        ),
        check_vma=False,
    )
```

time: 227 us -> 185 us (0.81)
  other arithmetic: 96 us -> 3.92 us
  Pallas kernels: 0 us -> 83.1 us
  matrix products: 43.1 us -> 0 us
  waiting for transfers between devices: 1.8 us -> 6.09 us
  blocking collectives: 63.3 us -> 66.4 us
  local copies, waits for them, and re-layouts: 2.41 us -> 4.71 us
    pallas_call x0 -> x3, Pallas kernels: none -> 83.1 us  [the longest x1 30.9 us: on_device(): pl.pallas_call(functools.partial(backward_kernel, total_chans), grid=(seq...]
    reduce_sum x3 -> x0, other arithmetic: 68.9 us -> none  [the longest x2 49.5 us: on_device(): jnp.sum(conv_grad * padded[:, tap_index:tap_index + tok_rows], axis=(0, 1))]
    dot_general x2 -> x0, matrix products: 43.1 us -> none  [the longest x1 23.3 us: on_device(): lax.dot_general(flat_swished, flat_cot, (((0,), (0,)), ((), ())), preferr...]
    add x2 -> x0, other arithmetic: 17.3 us -> none  [the longest x1 16.2 us: on_device(): spread + tap_rows[tap_index] * wide_grad[:, begin:begin + tok_rows + reach]]
    convert_element_type x5 -> x1, other arithmetic: 9.82 us -> 0.93 us  [on_device(): tail = (values_in[:, tokens - HALO:].astype(F32) * tail_sig).astype(BF16)]
    ppermute x2, waiting for transfers between devices: 1.79 us -> 6.07 us  [passed_along(): return lax.ppermute(shard, axis, pairs)]
    psum x3, blocking collectives: 63.3 us -> 66.4 us  [the longest x1 44 us: on_device(): small = lax.psum(small, 'sp')]
  transfers between devices with their start and end apart: 3 -> 3, of which waited for: 1 -> 1; matrix products, arithmetic and copies ran while one was open for 42% -> 3% of each run, Pallas kernels for 0% -> 17%
where the time goes in v1:
time: 185 us
  Pallas kernels  83.1 us (45%)
  blocking collectives  66.4 us (36%)
  between operations  14.1 us (8%)
  starting transfers between devices  6.23 us (3%)
  waiting for transfers between devices  6.09 us (3%)
  local copies, waits for them, and re-layouts  4.71 us (3%)
  other arithmetic  3.92 us (2%)
    psum x1, blocking collectives, on_device(): small = lax.psum(small, 'sp')  44 us
    pallas_call x1, Pallas kernels, on_device(): pl.pallas_call(functools.partial(backward_kernel, total_chans), grid=(seq...  30.9 us
    pallas_call x1, Pallas kernels, on_device(): pl.pallas_call(functools.partial(forward_kernel, seq_blocks), grid=(block...  27.1 us
    pallas_call x1, Pallas kernels, on_device(): pl.pallas_call(functools.partial(middle_kernel, blocks, total_chans), gri...  25.1 us
    psum x1, blocking collectives, on_device(): stats = lax.psum(sums, 'tp')  12.1 us
    psum x1, blocking collectives, on_device(): back = lax.psum(back, 'tp')  10.4 us
    ppermute x2, starting transfers between devices, passed_along(): return lax.ppermute(shard, axis, pairs)  6.19 us
    ppermute x2, waiting for transfers between devices, passed_along(): return lax.ppermute(shard, axis, pairs)  6.07 us
  transfers between devices with their start and end apart: 3, of which 1 were waited for; matrix products, arithmetic and copies ran while one was open for 3% of the time, Pallas kernels for 17%

profile of v1, /device:TPU:0, one launch (start us, length us, event | category | flops | bytes accessed | tf_op | source)
XLA Modules:
  0.0 184.7 jit_solution(8884460965379150916)
XLA Ops:
  7.2 0.0 reduce-scatter.2.cloned.1.call-start
  7.2 0.9 multiply_convert_fusion
  8.1 4.9 %collective-permute-start = (bf16[4,32,256]{2,1,0:T(8,128)(2,1)S(1)}, bf16[4,32,256]{2,1,0:T(8,128)(2,1)S(1)}, u32[]{:S(2)}, u32[]{:S(2)}) collective-permute-start(bf16[4,32,256]{2,1,0:T(8,128)(2,1)S(1)} %multiply_convert_fusion), channel_id=1, source_target_pairs={{0,4},{4,8},{8,12},{12,16},{16,20},{20,24},{24,28},{1,5},{5,9},{9,... | collective-permute-start | bytes 196616 | tf_op jit(solution)/shard_map/ppermute | solution.py:26
  13.0 0.7 bitcast_convert_fusion
  13.7 1.2 broadcast_in_dim.32
  14.9 0.7 reshape.54
  15.7 0.0 collective-permute-done.halo_ref
  15.7 0.0 copy-start.2
  15.7 0.6 squeeze.9.bias_ref
  16.3 0.7 broadcast_in_dim.25.taps_ref
  17.0 27.1 %forward.1 = (f32[4096,256]{1,0:T(8,128)}, f32[4096,256]{1,0:T(8,128)}, f32[2,32,128]{2,1,0:T(8,128)}) custom-call(bf16[4096,256]{1,0:T(8,128)(2,1)} %bitcast.29, bf16[4096,256]{1,0:T(8,128)(2,1)} %bitcast.31, bf16[4,32,256]{2,1,0:T(8,128)(2,1)} %copy-done.2, f32[2,31,8,128]{3,2,1,0:T(8,128)} %broadcast_in_dim.25.taps_ref, f32[2,8,128]{2,1,0:T(8,128)} %squeeze.9.bias_ref, ...), custom_call_target="tpu_custom_call" | custom-call | tf_op jit(solution)/shard_map/forward/pallas_call | solution.py:291
  44.1 12.1 %psum.21.stats_ref = f32[2,32,128]{2,1,0:T(8,128)} all-reduce(f32[2,32,128]{2,1,0:T(8,128)} %get-tuple-element.16), channel_id=1, replica_groups=mesh['sp'=8,'tp'=4] {'tp'}, use_global_device_ids=true, to_apply=%region_0.0 | all-reduce | flops 8192 | bytes 65536 | tf_op jit(solution)/shard_map/psum | solution.py:313
  56.2 25.1 %middle.1 = (f32[4096,256]{1,0:T(8,128)}, f32[2,32,128]{2,1,0:T(8,128)}, f32[8,256]{1,0:T(8,128)}, f32[256,4096]{1,0:T(8,128)}) custom-call(f32[4096,256]{1,0:T(8,128)} %get-tuple-element.17.conv_ref, f32[4096,256]{1,0:T(8,128)} %get-tuple-element.18.grad_ref, f32[2,32,128]{2,1,0:T(8,128)} %psum.21.stats_ref, f32[1,256]{1,0:T(1,128)} %bitcast.35, ...), custom_call_target="tpu_custom_call" | custom-call | tf_op jit(solution)/shard_map/middle/pallas_call | solution.py:316
  81.3 0.0 reduce-scatter.2.cloned.1.call-update
  81.4 0.7 copy-done
  82.1 10.4 %psum.22.back_ref = f32[2,32,128]{2,1,0:T(8,128)S(1)} all-reduce(f32[2,32,128]{2,1,0:T(8,128)S(1)} %copy-done.4), channel_id=1, replica_groups=mesh['sp'=8,'tp'=4] {'tp'}, use_global_device_ids=true, to_apply=%region_1.0 | all-reduce | flops 8192 | bytes 65536 | tf_op jit(solution)/shard_map/psum | solution.py:342
  92.6 1.1 fusion.3
  93.7 1.3 collective-permute-start.1
  95.0 6.1 %collective-permute-done.1.next_ref = f32[4,32,256]{2,1,0:T(8,128)S(1)} collective-permute-done((f32[4,32,256]{2,1,0:T(8,128)S(1)}, f32[4,32,256]{2,1,0:T(8,128)S(1)}, u32[]{:S(2)}, u32[]{:S(2)}) %collective-permute-start.1) | collective-permute-done | bytes 131104 | tf_op jit(solution)/shard_map/ppermute | solution.py:26
  101.1 0.6 copy-done.3
  101.7 30.9 %backward.1 = (bf16[4096,256]{1,0:T(8,128)(2,1)}, bf16[4096,256]{1,0:T(8,128)(2,1)}, f32[40,256]{1,0:T(8,128)}) custom-call(bf16[4096,256]{1,0:T(8,128)(2,1)} %bitcast.30, bf16[4096,256]{1,0:T(8,128)(2,1)} %bitcast.32, bf16[4,32,256]{2,1,0:T(8,128)(2,1)} %copy-done.2, f32[4,32,256]{2,1,0:T(8,128)} %copy-done.3, f32[2,31,8,128]{3,2,1,0:T(8,128)} %broadcast_in_dim.25.taps_ref, ...), custom_call_target="tpu_custom_call" | custom-call | tf_op jit(solution)/shard_map/backward/pallas_call | solution.py:363
  132.6 44.0 %psum.23 = f32[40,256]{1,0:T(8,128)S(1)} all-reduce(f32[40,256]{1,0:T(8,128)} %get-tuple-element.24), channel_id=1, replica_groups=mesh['sp'=8,'tp'=4] {'sp'}, use_global_device_ids=true, to_apply=%region_2.0 | all-reduce | flops 10240 | bytes 81920 | tf_op jit(solution)/shard_map/psum | solution.py:393
  176.6 0.6 slice.70
  177.2 0.6 fusion.11
  (17 shorter events, 0.1 us)
Async XLA Ops:
  7.2 170.7 %reduce-scatter.2.cloned.1.call-start = ((), (), s32[]{:S(2)}) async-start(), calls=%async_computation.1 | async-start | bytes 4718592 | tf_op jit(solution)/shard_map/reduce_scatter | solution.py:343
  8.1 7.5 %collective-permute-start = (bf16[4,32,256]{2,1,0:T(8,128)(2,1)S(1)}, bf16[4,32,256]{2,1,0:T(8,128)(2,1)S(1)}, u32[]{:S(2)}, u32[]{:S(2)}) collective-permute-start(bf16[4,32,256]{2,1,0:T(8,128)(2,1)S(1)} %multiply_convert_fusion), channel_id=1, source_target_pairs={{0,4},{4,8},{8,12},{12,16},{16,20},{20,24},{24,28},{1,5},{5,9},{9,... | collective-permute-start | bytes 196616 | tf_op jit(solution)/shard_map/ppermute | solution.py:26
  15.7 1.3 copy-start.2
  81.3 0.8 copy-start
  81.3 0.8 copy-start.4
  92.5 8.6 %copy-start.1 = (f32[2,32,128]{2,1,0:T(8,128)}, f32[2,32,128]{2,1,0:T(8,128)S(1)}, u32[]{:S(2)}) copy-start(f32[2,32,128]{2,1,0:T(8,128)S(1)} %psum.22.back_ref) | copy-start | bytes 98308
  93.7 7.4 %collective-permute-start.1 = (f32[4,32,256]{2,1,0:T(8,128)S(1)}, f32[4,32,256]{2,1,0:T(8,128)S(1)}, u32[]{:S(2)}, u32[]{:S(2)}) collective-permute-start(f32[4,32,256]{2,1,0:T(8,128)S(1)} %fusion.3), channel_id=1, source_target_pairs={{4,0},{8,4},{12,8},{16,12},{20,16},{24,20},{28,24},{5,1},{9,5},{13... | collective-permute-start | bytes 393224 | tf_op jit(solution)/shard_map/ppermute | solution.py:26
  101.1 0.6 copy-start.3
Sparse Core Ops, SparseCore 0:
  81.5 91.6 reduce-scatter.1

commit v2 on v1

v2 whole, which is shorter than its diff:
```python
import functools

import jax
import jax.numpy as jnp
from jax import lax
from jax.experimental import pallas as pl
from jax.experimental.pallas import tpu as pltpu
from jax.sharding import PartitionSpec as P

K = 31
EPS = 1e-05
HALO = 32
LANES = 128
F32 = jnp.float32
BF16 = jnp.bfloat16
VMEM_LIMIT = 60 * 1024 * 1024


def sigmoid(x):
    return 0.5 * jnp.tanh(0.5 * x) + 0.5


def peer_id(axis, distance):
    devices = lax.axis_size(axis)
    return {axis: lax.rem(lax.axis_index(axis) + distance, devices)}


def greet(pairs):
    barrier = pltpu.get_barrier_semaphore()
    for axis, distance in pairs:
        pl.semaphore_signal(
            barrier, inc=1, device_id=peer_id(axis, distance),
            device_id_type=pl.DeviceIdType.MESH,
        )
    pl.semaphore_wait(barrier, len(pairs))


def remote(src, dst, send_sem, recv_sem, axis, distance):
    return pltpu.make_async_remote_copy(
        src_ref=src, dst_ref=dst, send_sem=send_sem, recv_sem=recv_sem,
        device_id=peer_id(axis, distance), device_id_type=pl.DeviceIdType.MESH,
    )


def fir(x_ref, w_ref, lane_block, start, taps, blocks, init):
    accs = [init] * blocks
    x_block, w_block = lane_block
    weights = [w_ref[w_block, k] for k in taps]
    for offset in range(K + 8 * (blocks - 1)):
        piece = x_ref[x_block, pl.ds(start + offset, 8), :]
        for a in range(blocks):
            k = offset - 8 * a
            if 0 <= k < K:
                term = weights[k] * piece
                accs[a] = term if accs[a] is None else accs[a] + term
    return accs


def lane_sums(x):
    return jnp.sum(x.T, axis=0, keepdims=True)


def row_spread(row):
    return jnp.broadcast_to(row, (LANES, LANES)).T


def forward_kernel(
    seqs, seq_blocks, values_ref, gates_ref, values_before_ref, gates_before_ref, values_hbm,
    gates_hbm, taps_ref, bias_ref, cot_ref, weight_ref,
    conv_ref, grad_ref, sums_ref, halo_ref, padded, values_halo, gates_halo, send_sems, recv_sems,
):
    step = pl.program_id(0)
    rows, chans = values_ref.shape
    lane_blocks = chans // LANES
    chunks = rows // LANES
    depth = cot_ref.shape[1] // chunks
    seq = lax.rem(step, seqs)
    part = seq_blocks - 1 - step // seqs
    block = seq * seq_blocks + part
    sp_devices = lax.axis_size("sp")
    tail = pl.ds(values_hbm.shape[1] - HALO, HALO)
    copies = [
        remote(src.at[:, tail], dst, send_sems.at[n], recv_sems.at[n], "sp", 1)
        for n, (src, dst) in enumerate(((values_hbm, values_halo), (gates_hbm, gates_halo)))
    ]

    @pl.when(step == 0)
    def _():
        greet((("sp", 1), ("sp", sp_devices - 1)))
        for copy in copies:
            copy.start()

    @pl.when(step == seqs * (seq_blocks - 1))
    def _():
        for copy in copies:
            copy.wait()

    grad_ref[...] = jnp.zeros_like(grad_ref)

    def fill(values, gates, keep):
        for h in range(lane_blocks):
            lanes = slice(h * LANES, (h + 1) * LANES)
            sig = sigmoid(gates[:, lanes].astype(F32))
            gated = (values[:, lanes].astype(F32) * sig).astype(BF16).astype(F32)
            padded[h, :HALO, :] = gated * keep

    @pl.when(part == 0)
    def _():
        keep = jnp.where(lax.axis_index("sp") > 0, 1.0, 0.0).astype(F32)
        fill(values_halo[seq], gates_halo[seq], keep)
        for h in range(lane_blocks):
            halo_ref[seq, :, h * LANES : (h + 1) * LANES] = padded[h, :HALO, :]

    @pl.when(part != 0)
    def _():
        fill(values_before_ref[...], gates_before_ref[...], 1.0)

    def chunk(i, carry):
        first = pl.multiple_of(i * LANES, LANES)
        here = pl.ds(first, LANES)
        columns = pl.ds(pl.multiple_of(i * depth, depth), depth)
        grad_ref[...] += lax.dot_general(
            cot_ref[:, columns], weight_ref[:, columns], (((1,), (1,)), ((), ())),
            preferred_element_type=F32,
        )
        total = None
        for h in range(lane_blocks):
            lanes = slice(h * LANES, (h + 1) * LANES)
            sig = sigmoid(gates_ref[here, lanes].astype(F32))
            gated = (values_ref[here, lanes].astype(F32) * sig).astype(BF16).astype(F32)
            padded[h, pl.ds(first + HALO, LANES), :] = gated
            for c in range(LANES // 32):
                start = first + c * 32
                accs = fir(padded, taps_ref, (h, h), start + HALO - K + 1, range(K), 4, bias_ref[h])
                for a in range(4):
                    conv_ref[pl.ds(pl.multiple_of(start + 8 * a, 8), 8), lanes] = accs[a]
        total = square = None
        for h in range(lane_blocks):
            conv = conv_ref[here, h * LANES : (h + 1) * LANES]
            total = conv if total is None else total + conv
            square = conv * conv if square is None else square + conv * conv
        row = block * chunks + i
        sums_ref[0, pl.ds(row, 1), :] = lane_sums(total)
        sums_ref[1, pl.ds(row, 1), :] = lane_sums(square)
        return carry

    lax.fori_loop(0, chunks, chunk, 0)


def middle_kernel(
    blocks, total_chans, conv_ref, grad_ref, own_sums_ref, own_sums_hbm, gain_ref, cot_ref,
    normed_grad_ref, sums_ref, gain_grad_ref, weight_out_ref, stats_ref,
    swished, weight_grad_ref, arrived, send_sems, recv_sems,
):
    step = pl.program_id(0)
    rows, chans = conv_ref.shape
    lane_blocks = chans // LANES
    chunks = rows // LANES
    width = cot_ref.shape[1] // chunks
    now = lax.rem(step, 2)
    before = 1 - now

    @pl.when(step == 0)
    def _():
        peers = range(1, lax.axis_size("tp"))
        greet([("tp", d) for d in peers])
        copies = [
            remote(
                own_sums_hbm, arrived.at[d - 1], send_sems.at[d - 1], recv_sems.at[d - 1], "tp", d
            )
            for d in peers
        ]
        for copy in copies:
            copy.start()
        weight_grad_ref[...] = jnp.zeros_like(weight_grad_ref)
        gain_grad_ref[...] = jnp.zeros_like(gain_grad_ref)
        swished[1] = jnp.zeros(swished.shape[1:], BF16)
        total = own_sums_ref[...]
        for d, copy in zip(peers, copies):
            copy.wait()
            total = total + arrived[d - 1]
        stats_ref[...] = total

    fresh = jnp.where(step < blocks, 1.0, 0.0).astype(F32)
    block = jnp.minimum(step, blocks - 1)

    def chunk(i, carry):
        first = pl.multiple_of(i * LANES, LANES)
        here = pl.ds(first, LANES)
        columns = pl.ds(pl.multiple_of(i * width, width), width)
        weight_grad_ref[:, columns] += jnp.dot(
            swished[before], cot_ref[:, columns], preferred_element_type=F32
        )
        row = block * chunks + i
        mean = stats_ref[0, pl.ds(row, 1), :] / total_chans
        variance = stats_ref[1, pl.ds(row, 1), :] / total_chans - mean * mean
        inverse = row_spread(lax.rsqrt(variance + EPS))
        mean = row_spread(mean)
        plain = weighted = None
        for h in range(lane_blocks):
            lanes = slice(h * LANES, (h + 1) * LANES)
            gain = gain_ref[:, lanes]
            normed = (conv_ref[here, lanes] - mean) * inverse
            scaled = normed * gain
            sig = sigmoid(scaled)
            silu = scaled * sig
            swished[now, lanes, here] = silu.T.astype(BF16)
            scaled_grad = grad_ref[here, lanes] * (sig + silu * (1.0 - sig))
            normed_grad = scaled_grad * gain
            normed_grad_ref[here, lanes] = normed_grad
            product = scaled_grad * normed
            gain_grad_ref[:, lanes] += fresh * jnp.sum(
                product.reshape(LANES // 8, 8, LANES), axis=0
            )
            product = product * gain
            plain = normed_grad if plain is None else plain + normed_grad
            weighted = product if weighted is None else weighted + product
        sums_ref[0, pl.ds(row, 1), :] = lane_sums(plain)
        sums_ref[1, pl.ds(row, 1), :] = lane_sums(weighted)
        return carry

    lax.fori_loop(0, chunks, chunk, 0)

    @pl.when(step == blocks)
    def _():
        weight_out_ref[...] = weight_grad_ref[...].astype(BF16)


def backward_kernel(
    total_chans, seqs, values_hbm, gates_hbm, conv_hbm, normed_grad_hbm, weight_hbm, back_hbm,
    halo_ref, taps_ref, stats_ref, own_back_ref, gain_grad_ref,
    values_grad_hbm, gates_grad_hbm, small_ref, weight_grad_ref,
    values, gates, conv, normed_grad, padded, wide, heads, back, back_arrived, small,
    small_arrived, own_weight, weight_arrived, local_sems, out_sems, weight_sem,
    back_send, back_recv, weight_send, weight_recv, head_send, head_recv, small_send, small_recv,
):
    positions, chans = values.shape
    tokens = positions // seqs
    lane_blocks = chans // LANES
    chunks = tokens // LANES
    sp_devices = lax.axis_size("sp")
    me = lax.axis_index("sp")
    tp_peers = range(1, lax.axis_size("tp"))
    sp_peers = range(1, sp_devices)

    def rows_of(s):
        return pl.ds(s * tokens, tokens)

    loads = []
    for s in range(seqs):
        pairs = ((values_hbm, values), (gates_hbm, gates), (conv_hbm, conv),
                 (normed_grad_hbm, normed_grad))
        loads.append([
            pltpu.make_async_copy(src.at[rows_of(s)], dst.at[rows_of(s)], local_sems.at[s, n])
            for n, (src, dst) in enumerate(pairs)
        ])
        for copy in loads[s]:
            copy.start()
    greet([("tp", d) for d in tp_peers] + [("sp", d) for d in sp_peers])
    back_copies = [
        remote(back_hbm, back_arrived.at[d - 1], back_send.at[d - 1], back_recv.at[d - 1], "tp", d)
        for d in tp_peers
    ]
    for copy in back_copies:
        copy.start()
    weight_copies = [
        remote(
            weight_hbm.at[lax.rem(me + d, sp_devices)], weight_arrived.at[d - 1],
            weight_send.at[d - 1], weight_recv.at[d - 1], "sp", d,
        )
        for d in sp_peers
    ]
    for copy in weight_copies:
        copy.start()
    own_copy = pltpu.make_async_copy(weight_hbm.at[me], own_weight, weight_sem)
    own_copy.start()

    total = own_back_ref[...]
    for d, copy in zip(tp_peers, back_copies):
        copy.wait()
        total = total + back_arrived[d - 1]
    back[...] = total

    for s in range(seqs):
        for h in range(lane_blocks):
            padded[s * lane_blocks + h, :HALO, :] = halo_ref[s, :, h * LANES : (h + 1) * LANES]
    bias_accs = tuple(jnp.zeros((8, LANES), F32) for _ in range(lane_blocks))
    for s in range(seqs):
        for copy in loads[s]:
            copy.wait()

        def prepare(i, accs):
            accs = list(accs)
            first = pl.multiple_of(i * LANES, LANES)
            here = pl.ds(s * tokens + first, LANES)
            row = s * chunks + i
            mean = stats_ref[0, pl.ds(row, 1), :] / total_chans
            variance = stats_ref[1, pl.ds(row, 1), :] / total_chans - mean * mean
            inverse = row_spread(lax.rsqrt(variance + EPS))
            mean = row_spread(mean)
            plain = row_spread(back[0, pl.ds(row, 1), :] / total_chans)
            weighted = row_spread(back[1, pl.ds(row, 1), :] / total_chans)
            for h in range(lane_blocks):
                lanes = slice(h * LANES, (h + 1) * LANES)
                sig = sigmoid(gates[here, lanes].astype(F32))
                gated = (values[here, lanes].astype(F32) * sig).astype(BF16).astype(F32)
                padded[s * lane_blocks + h, pl.ds(first + HALO, LANES), :] = gated
                normed = (conv[here, lanes] - mean) * inverse
                conv_grad = inverse * (normed_grad[here, lanes] - plain - normed * weighted)
                wide[s * lane_blocks + h, pl.ds(first, LANES), :] = conv_grad
                accs[h] = accs[h] + jnp.sum(conv_grad.reshape(LANES // 8, 8, LANES), axis=0)
            return tuple(accs)

        bias_accs = lax.fori_loop(0, chunks, prepare, bias_accs)

    head_copy = remote(
        wide.at[:, pl.ds(0, HALO)], heads, head_send, head_recv, "sp", sp_devices - 1
    )
    head_copy.start()

    for h in range(lane_blocks):
        accs = tuple(jnp.zeros((8, LANES), F32) for _ in range(K))
        for s in range(seqs):
            where = s * lane_blocks + h

            def correlate(i, accs):
                start = pl.multiple_of(i * 32, 32)
                accs = list(accs)
                grads = [
                    wide[where, pl.ds(pl.multiple_of(start + 8 * a, 8), 8), :] for a in range(4)
                ]
                for offset in range(K + 24):
                    piece = padded[where, pl.ds(start + HALO - K + 1 + offset, 8), :]
                    for a in range(4):
                        k = offset - 8 * a
                        if 0 <= k < K:
                            accs[k] = accs[k] + grads[a] * piece
                return tuple(accs)

            accs = lax.fori_loop(0, tokens // 32, correlate, accs)
        lanes = slice(h * LANES, (h + 1) * LANES)
        for k in range(K):
            small[k : k + 1, lanes] = jnp.sum(accs[k], axis=0, keepdims=True)
        small[K : K + 1, lanes] = jnp.sum(bias_accs[h], axis=0, keepdims=True)
        small[K + 1 : K + 2, lanes] = jnp.sum(gain_grad_ref[:, lanes], axis=0, keepdims=True)
        small[K + 2 :, lanes] = jnp.zeros((small.shape[0] - K - 2, LANES), F32)

    small_copies = [
        remote(small, small_arrived.at[d - 1], small_send.at[d - 1], small_recv.at[d - 1], "sp", d)
        for d in sp_peers
    ]

    def spread_chunk(s, start):
        here = pl.ds(pl.multiple_of(s * tokens + start, 32), 32)
        for h in range(lane_blocks):
            lanes = slice(h * LANES, (h + 1) * LANES)
            accs = fir(
                wide, taps_ref, (s * lane_blocks + h, h), start, range(K - 1, -1, -1), 4, None
            )
            gated_grad = jnp.concatenate(accs, axis=0)
            sig = sigmoid(gates[here, lanes].astype(F32))
            values_part = gated_grad * sig
            gates_part = values_part * values[here, lanes].astype(F32) * (1.0 - sig)
            values[here, lanes] = values_part.astype(BF16)
            gates[here, lanes] = gates_part.astype(BF16)

    for s in range(seqs):

        def spread(i, carry):
            spread_chunk(s, pl.multiple_of(i * 32, 32))
            return carry

        lax.fori_loop(0, tokens // 32 - 1, spread, 0)
        if s == 0:
            for copy in small_copies:
                copy.start()

    head_copy.wait()
    keep = jnp.where(me < sp_devices - 1, 1.0, 0.0).astype(F32)
    stores = []
    for s in range(seqs):
        for h in range(lane_blocks):
            where = s * lane_blocks + h
            wide[where, tokens:, :] = heads[where] * keep
        spread_chunk(s, tokens - 32)
        for n, (src, dst) in enumerate(((values, values_grad_hbm), (gates, gates_grad_hbm))):
            copy = pltpu.make_async_copy(
                src.at[rows_of(s)], dst.at[rows_of(s)], out_sems.at[s, n]
            )
            copy.start()
            stores.append(copy)

    own_copy.wait()
    weight_grad_ref[...] = own_weight[...].astype(F32)
    for d, copy in zip(sp_peers, weight_copies):
        copy.wait()
        weight_grad_ref[...] += weight_arrived[d - 1].astype(F32)
    sum_small = small[...]
    for d, copy in zip(sp_peers, small_copies):
        copy.wait()
        sum_small = sum_small + small_arrived[d - 1]
    small_ref[...] = sum_small
    for copy in stores:
        copy.wait()


def whole(shape):
    return pl.BlockSpec(shape, lambda i: (0,) * len(shape))


def on_device(values_in, gates_in, conv_taps, conv_bias, norm_gain, out_weight, out_grad):
    seqs, tokens, chans = values_in.shape
    width = out_grad.shape[2]
    total_chans = chans * lax.axis_size("tp")
    lane_blocks = chans // LANES
    positions = seqs * tokens
    rows = min(512, tokens)
    blocks = positions // rows
    stat_rows = positions // LANES

    values = values_in.reshape(positions, chans)
    gates = gates_in.reshape(positions, chans)
    cot = out_grad.reshape(positions, width)

    def by_lanes(rows_of):
        count = rows_of.shape[0]
        split = rows_of.astype(F32).reshape(count, lane_blocks, 1, LANES).transpose(1, 0, 2, 3)
        return jnp.broadcast_to(split, (lane_blocks, count, 8, LANES))

    taps8 = by_lanes(conv_taps)
    bias8 = by_lanes(conv_bias[None])[:, 0]
    gain = norm_gain.astype(F32)[None]

    tp_others = lax.axis_size("tp") - 1
    sp_devices = lax.axis_size("sp")
    sp_others = sp_devices - 1

    def params(ident):
        return pltpu.CompilerParams(
            dimension_semantics=("arbitrary",), vmem_limit_bytes=VMEM_LIMIT,
            collective_id=ident, has_side_effects=True,
        )

    def dma(*shape):
        return pltpu.SemaphoreType.DMA(shape)

    anywhere = pl.BlockSpec(memory_space=pl.ANY)
    stats_shape = (2, stat_rows, LANES)
    seq_blocks = tokens // rows

    def block_of(i):
        return i % seqs * seq_blocks + seq_blocks - 1 - i // seqs

    tile = pl.BlockSpec((rows, chans), lambda i: (block_of(i), 0))
    ahead_halo = pl.BlockSpec(
        (HALO, chans), lambda i: (jnp.maximum(block_of(i) * (rows // HALO) - 1, 0), 0)
    )
    conv, swish_grad, sums, halo = pl.pallas_call(
        functools.partial(forward_kernel, seqs, seq_blocks),
        grid=(blocks,),
        in_specs=[
            tile, tile, ahead_halo, ahead_halo, anywhere, anywhere,
            whole(taps8.shape),
            whole(bias8.shape),
            pl.BlockSpec((rows, width), lambda i: (block_of(i), 0)),
            whole(out_weight.shape),
        ],
        out_specs=[tile, tile, whole(stats_shape), whole((seqs, HALO, chans))],
        out_shape=[
            jax.ShapeDtypeStruct((positions, chans), F32),
            jax.ShapeDtypeStruct((positions, chans), F32),
            jax.ShapeDtypeStruct(stats_shape, F32),
            jax.ShapeDtypeStruct((seqs, HALO, chans), F32),
        ],
        scratch_shapes=[
            pltpu.VMEM((lane_blocks, rows + HALO, LANES), F32),
            pltpu.VMEM((seqs, HALO, chans), BF16),
            pltpu.VMEM((seqs, HALO, chans), BF16),
            dma(2),
            dma(2),
        ],
        compiler_params=params(0),
        name="forward",
    )(values, gates, values, gates, values_in, gates_in, taps8, bias8, cot, out_weight)

    ahead = pl.BlockSpec((rows, chans), lambda i: (jnp.minimum(i, blocks - 1), 0))
    normed_grad, back, gain_local, weight_local, stats = pl.pallas_call(
        functools.partial(middle_kernel, blocks, total_chans),
        grid=(blocks + 1,),
        in_specs=[
            ahead,
            ahead,
            whole(stats_shape),
            anywhere,
            whole((1, chans)),
            pl.BlockSpec((rows, width), lambda i: (jnp.maximum(i - 1, 0), 0)),
        ],
        out_specs=[
            ahead,
            whole(stats_shape),
            whole((8, chans)),
            whole((chans, width)),
            whole(stats_shape),
        ],
        out_shape=[
            jax.ShapeDtypeStruct((positions, chans), F32),
            jax.ShapeDtypeStruct(stats_shape, F32),
            jax.ShapeDtypeStruct((8, chans), F32),
            jax.ShapeDtypeStruct((chans, width), BF16),
            jax.ShapeDtypeStruct(stats_shape, F32),
        ],
        scratch_shapes=[
            pltpu.VMEM((2, chans, rows), BF16),
            pltpu.VMEM((chans, width), F32),
            pltpu.VMEM((tp_others, *stats_shape), F32),
            dma(tp_others),
            dma(tp_others),
        ],
        compiler_params=params(1),
        name="middle",
    )(conv, swish_grad, sums, sums, gain, cot)

    small_rows = -(-(K + 2) // 8) * 8
    weight_rows = chans // sp_devices
    padded_shape = (seqs * lane_blocks, tokens + HALO, LANES)
    values_grad, gates_grad, small, weight_grad = pl.pallas_call(
        functools.partial(backward_kernel, total_chans, seqs),
        in_specs=[anywhere] * 6 + [pl.BlockSpec(memory_space=pltpu.VMEM)] * 5,
        out_specs=[anywhere] * 2 + [pl.BlockSpec(memory_space=pltpu.VMEM)] * 2,
        out_shape=[
            jax.ShapeDtypeStruct((positions, chans), BF16),
            jax.ShapeDtypeStruct((positions, chans), BF16),
            jax.ShapeDtypeStruct((small_rows, chans), F32),
            jax.ShapeDtypeStruct((weight_rows, width), F32),
        ],
        scratch_shapes=[
            pltpu.VMEM((positions, chans), BF16),
            pltpu.VMEM((positions, chans), BF16),
            pltpu.VMEM((positions, chans), F32),
            pltpu.VMEM((positions, chans), F32),
            pltpu.VMEM(padded_shape, F32),
            pltpu.VMEM(padded_shape, F32),
            pltpu.VMEM((seqs * lane_blocks, HALO, LANES), F32),
            pltpu.VMEM(stats_shape, F32),
            pltpu.VMEM((tp_others, *stats_shape), F32),
            pltpu.VMEM((small_rows, chans), F32),
            pltpu.VMEM((sp_others, small_rows, chans), F32),
            pltpu.VMEM((weight_rows, width), BF16),
            pltpu.VMEM((sp_others, weight_rows, width), BF16),
            dma(seqs, 4),
            dma(seqs, 2),
            pltpu.SemaphoreType.DMA,
            dma(tp_others),
            dma(tp_others),
            dma(sp_others),
            dma(sp_others),
            pltpu.SemaphoreType.DMA,
            pltpu.SemaphoreType.DMA,
            dma(sp_others),
            dma(sp_others),
        ],
        compiler_params=pltpu.CompilerParams(
            vmem_limit_bytes=VMEM_LIMIT, collective_id=2, has_side_effects=True
        ),
        name="backward",
    )(
        values, gates, conv, normed_grad,
        weight_local.reshape(sp_devices, weight_rows, width), back,
        halo, taps8, stats, back, gain_local,
    )
    return (
        values_grad.reshape(values_in.shape),
        gates_grad.reshape(values_in.shape),
        small[:K],
        small[K + 1],
        small[K],
        weight_grad,
    )


def solution(mesh):
    return jax.shard_map(
        on_device,
        mesh=mesh,
        in_specs=(
            P(None, "sp", "tp"),
            P(None, "sp", "tp"),
            P(None, "tp"),
            P("tp"),
            P("tp"),
            P("tp", None),
            P(None, "sp", None),
        ),
        out_specs=(
            P(None, "sp", "tp"),
            P(None, "sp", "tp"),
            P(None, "tp"),
            P("tp"),
            P("tp"),
            P(("tp", "sp"), None),
        ),
        check_vma=False,
    )
```

time: 185 us -> 135 us (0.73)
  blocking collectives: 66.4 us -> 0 us
  Pallas kernels: 83.1 us -> 122 us
  between operations: 14.1 us -> 0.67 us
  starting transfers between devices: 6.23 us -> 0 us
  waiting for transfers between devices: 6.09 us -> 0 us
  local copies, waits for them, and re-layouts: 4.71 us -> 10.1 us
  other arithmetic: 3.92 us -> 1.88 us
    psum x3 -> x0, blocking collectives: 66.4 us -> none  [the longest x1 44 us: on_device(): small = lax.psum(small, 'sp')]
    pallas_call x2, Pallas kernels: 58 us -> 93 us  [the longest x1 59.4 us: on_device(): pl.pallas_call(functools.partial(backward_kernel, total_chans, seqs), in_...]
    ppermute x2 -> x0, starting transfers between devices: 6.19 us -> none  [passed_along(): return lax.ppermute(shard, axis, pairs)]
    ppermute x2 -> x0, waiting for transfers between devices: 6.07 us -> none  [passed_along(): return lax.ppermute(shard, axis, pairs)]
    unnamed x10 -> x7, local copies, waits for them, and re-layouts: 1.38 us -> 5.39 us
    pallas_call x1, Pallas kernels: 25.1 us -> 28.6 us  [on_device(): pl.pallas_call(functools.partial(middle_kernel, blocks, total_chans), gri...]
  transfers between devices with their start and end apart: 3 -> 0, of which waited for: 1 -> 0; matrix products, arithmetic and copies ran while one was open for 3% -> 0% of each run, Pallas kernels for 17% -> 0%
where the time goes in v2:
time: 135 us; the launch traced here: 134 us
  Pallas kernels  122 us (90%)
  local copies, waits for them, and re-layouts  10.1 us (7%)
  other arithmetic  1.88 us (1%)
    pallas_call x1, Pallas kernels, on_device(): pl.pallas_call(functools.partial(backward_kernel, total_chans, seqs), in_...  59.4 us
    pallas_call x1, Pallas kernels, on_device(): pl.pallas_call(functools.partial(forward_kernel, seqs, seq_blocks), grid=...  33.6 us
    pallas_call x1, Pallas kernels, on_device(): pl.pallas_call(functools.partial(middle_kernel, blocks, total_chans), gri...  28.6 us
    unnamed x7, local copies, waits for them, and re-layouts  5.39 us

profile of v2, /device:TPU:0, one launch (start us, length us, event | category | flops | bytes accessed | tf_op | source)
XLA Modules:
  0.0 134.2 jit_solution(15899535201133980642)
XLA Ops:
  0.6 0.7 bitcast_convert_fusion
  1.3 1.2 broadcast_in_dim.32
  2.5 0.6 squeeze.9.bias_ref
  3.1 0.7 reshape.50
  3.9 0.7 broadcast_in_dim.25.taps_ref
  4.6 33.6 %forward.1 = (f32[4096,256]{1,0:T(8,128)}, f32[4096,256]{1,0:T(8,128)}, f32[2,32,128]{2,1,0:T(8,128)}, f32[4,32,256]{2,1,0:T(8,128)}) custom-call(bf16[4096,256]{1,0:T(8,128)(2,1)} %bitcast.19, bf16[4096,256]{1,0:T(8,128)(2,1)} %bitcast.22, bf16[4096,256]{1,0:T(8,128)(2,1)} %bitcast.20, bf16[4096,256]{1,0:T(8,128)(2,1)} %bitcast.23, ...), custom_call_target="tpu_custom_call" | custom-call | tf_op jit(solution)/shard_map/forward/pallas_call | solution.py:458
  38.2 28.6 %middle.1 = (f32[4096,256]{1,0:T(8,128)}, f32[2,32,128]{2,1,0:T(8,128)}, f32[8,256]{1,0:T(8,128)}, bf16[256,4096]{1,0:T(8,128)(2,1)}, f32[2,32,128]{2,1,0:T(8,128)}) custom-call(f32[4096,256]{1,0:T(8,128)} %get-tuple-element.19.conv_ref.conv_hbm, f32[4096,256]{1,0:T(8,128)} %get-tuple-element.20.grad_ref, ...), custom_call_target="tpu_custom_call" | custom-call | tf_op jit(solution)/shard_map/middle/pallas_call | solution.py:487
  66.8 59.4 %backward.1 = (bf16[4096,256]{1,0:T(8,128)(2,1)}, bf16[4096,256]{1,0:T(8,128)(2,1)}, f32[40,256]{1,0:T(8,128)}, f32[32,4096]{1,0:T(8,128)}) custom-call(bf16[4096,256]{1,0:T(8,128)(2,1)} %bitcast.21, bf16[4096,256]{1,0:T(8,128)(2,1)} %bitcast.24, f32[4096,256]{1,0:T(8,128)} %get-tuple-element.19.conv_ref.conv_hbm, ...), custom_call_target="tpu_custom_call" | custom-call | tf_op jit(solution)/shard_map/backward/pallas_call | solution.py:526
  126.2 1.3 fusion
  127.5 1.4 %slice.9 = f32[31,256]{1,0:T(8,128)} slice(f32[40,256]{1,0:T(8,128)} %get-tuple-element.30), slice={[0:31], [0:256]} | slice | bytes 63488 | tf_op jit(solution)/shard_map/slice | solution.py:574
  128.9 0.0 copy-start
  128.9 3.2 %copy.19 = bf16[4,1024,256]{2,1,0:T(8,128)(2,1)} copy(bf16[4,1024,256]{2,1,0:T(8,128)(2,1)} %bitcast.26) | data formatting | bytes 4194304
  132.0 0.0 copy-done
  132.1 0.0 copy-start.1
  132.1 1.3 copy.20
  133.4 0.1 copy-done.1
  133.4 0.8 copy.21
  (1 shorter events, 0.0 us)
Async XLA Ops:
  128.9 3.2 %copy-start = (bf16[4096,256]{1,0:T(8,128)(2,1)S(1)}, bf16[4096,256]{1,0:T(8,128)(2,1)}, u32[]{:S(2)}) copy-start(bf16[4096,256]{1,0:T(8,128)(2,1)} %get-tuple-element.29) | copy-start | bytes 6291460
  132.1 1.4 %copy-start.1 = (f32[32,4096]{1,0:T(8,128)S(1)}, f32[32,4096]{1,0:T(8,128)}, u32[]{:S(2)}) copy-start(f32[32,4096]{1,0:T(8,128)} %get-tuple-element.45) | copy-start | bytes 1572868

commit v3 on v2

--- a/solution.py
+++ b/solution.py
@@ -10,6 +10,7 @@
 K = 31
 EPS = 1e-05
 HALO = 32
+PAIR = 2
 LANES = 128
 F32 = jnp.float32
 BF16 = jnp.bfloat16
@@ -66,8 +67,8 @@
 
 def forward_kernel(
     seqs, seq_blocks, values_ref, gates_ref, values_before_ref, gates_before_ref, values_hbm,
-    gates_hbm, taps_ref, bias_ref, cot_ref, weight_ref,
-    conv_ref, grad_ref, sums_ref, halo_ref, padded, values_halo, gates_halo, send_sems, recv_sems,
+    gates_hbm, raw_taps_ref, bias_ref, cot_ref, weight_ref,
+    conv_ref, grad_ref, sums_ref, halo_ref, taps_ref, padded, values_halo, gates_halo, send_sems, recv_sems,
 ):
     step = pl.program_id(0)
     rows, chans = values_ref.shape
@@ -89,6 +90,12 @@
         greet((("sp", 1), ("sp", sp_devices - 1)))
         for copy in copies:
             copy.start()
+        rows_of_taps = raw_taps_ref[...].astype(F32)
+        for h in range(lane_blocks):
+            for k in range(K):
+                taps_ref[h, k] = jnp.broadcast_to(
+                    rows_of_taps[k : k + 1, h * LANES : (h + 1) * LANES], (8, LANES)
+                )
 
     @pl.when(step == seqs * (seq_blocks - 1))
     def _():
@@ -129,9 +136,10 @@
             sig = sigmoid(gates_ref[here, lanes].astype(F32))
             gated = (values_ref[here, lanes].astype(F32) * sig).astype(BF16).astype(F32)
             padded[h, pl.ds(first + HALO, LANES), :] = gated
+            bias = jnp.broadcast_to(bias_ref[:, lanes].astype(F32), (8, LANES))
             for c in range(LANES // 32):
                 start = first + c * 32
-                accs = fir(padded, taps_ref, (h, h), start + HALO - K + 1, range(K), 4, bias_ref[h])
+                accs = fir(padded, taps_ref, (h, h), start + HALO - K + 1, range(K), 4, bias)
                 for a in range(4):
                     conv_ref[pl.ds(pl.multiple_of(start + 8 * a, 8), 8), lanes] = accs[a]
         total = square = None
@@ -231,7 +239,8 @@
     halo_ref, taps_ref, stats_ref, own_back_ref, gain_grad_ref,
     values_grad_hbm, gates_grad_hbm, small_ref, weight_grad_ref,
     values, gates, conv, normed_grad, padded, wide, heads, back, back_arrived, small,
-    small_arrived, own_weight, weight_arrived, local_sems, out_sems, weight_sem,
+    small_arrived, own_weight, pair_arrived, weight_arrived, local_sems, out_sems, weight_sem,
+    pair_send, pair_recv,
     back_send, back_recv, weight_send, weight_recv, head_send, head_recv, small_send, small_recv,
 ):
     positions, chans = values.shape
@@ -263,17 +272,53 @@
     ]
     for copy in back_copies:
         copy.start()
-    weight_copies = [
-        remote(
-            weight_hbm.at[lax.rem(me + d, sp_devices)], weight_arrived.at[d - 1],
-            weight_send.at[d - 1], weight_recv.at[d - 1], "sp", d,
+    group = PAIR if sp_devices % PAIR == 0 else 1
+    groups = sp_devices // group
+    inner = lax.rem(me, group)
+    outer = me // group
+    order = list(range(1, groups)) + [0]
+    pair_copies, own_copies, weight_copies = {}, {}, {}
+    for d in order:
+        base = lax.rem(outer + d, groups) * group
+        own_copies[d] = pltpu.make_async_copy(
+            weight_hbm.at[base + inner], own_weight.at[d], weight_sem.at[d]
         )
-        for d in sp_peers
-    ]
-    for copy in weight_copies:
-        copy.start()
-    own_copy = pltpu.make_async_copy(weight_hbm.at[me], own_weight, weight_sem)
-    own_copy.start()
+        own_copies[d].start()
+        if group > 1:
+            pair_copies[d] = remote(
+                weight_hbm.at[base + 1 - inner], pair_arrived.at[d], pair_send.at[d],
+                pair_recv.at[d], "sp", sp_devices + 1 - 2 * inner,
+            )
+            pair_copies[d].start()
+        if d > 0:
+            weight_copies[d] = remote(
+                own_weight.at[d], weight_arrived.at[d - 1], weight_send.at[d - 1],
+                weight_recv.at[d - 1], "sp", d * group,
+            )
+
+    def pair_sum(d):
+        own_copies[d].wait()
+        total = own_weight[d].astype(F32)
+        if group > 1:
+            pair_copies[d].wait()
+            total = total + pair_arrived[d].astype(F32)
+        return total
+
+    slots = seqs * lane_blocks + seqs
+    todo = {}
+    for n, d in enumerate(order[:-1]):
+        at = min(1 + n * slots // groups, slots - 2)
+        todo.setdefault(at, []).append((True, d))
+        todo.setdefault(at + 1, []).append((False, d))
+    slot = [0]
+
+    def forward_slices():
+        for adds, d in todo.pop(slot[0], []):
+            if adds:
+                own_weight[d] = pair_sum(d).astype(BF16)
+            else:
+                weight_copies[d].start()
+        slot[0] += 1
 
     total = own_back_ref[...]
     for d, copy in zip(tp_peers, back_copies):
@@ -338,6 +383,7 @@
                 return tuple(accs)
 
             accs = lax.fori_loop(0, tokens // 32, correlate, accs)
+            forward_slices()
         lanes = slice(h * LANES, (h + 1) * LANES)
         for k in range(K):
             small[k : k + 1, lanes] = jnp.sum(accs[k], axis=0, keepdims=True)
@@ -371,10 +417,13 @@
             return carry
 
         lax.fori_loop(0, tokens // 32 - 1, spread, 0)
+        forward_slices()
         if s == 0:
             for copy in small_copies:
                 copy.start()
 
+    while todo:
+        forward_slices()
     head_copy.wait()
     keep = jnp.where(me < sp_devices - 1, 1.0, 0.0).astype(F32)
     stores = []
@@ -390,9 +439,8 @@
             copy.start()
             stores.append(copy)
 
-    own_copy.wait()
-    weight_grad_ref[...] = own_weight[...].astype(F32)
-    for d, copy in zip(sp_peers, weight_copies):
+    weight_grad_ref[...] = pair_sum(0)
+    for d, copy in weight_copies.items():
         copy.wait()
         weight_grad_ref[...] += weight_arrived[d - 1].astype(F32)
     sum_small = small[...]
@@ -422,13 +470,6 @@
     gates = gates_in.reshape(positions, chans)
     cot = out_grad.reshape(positions, width)
 
-    def by_lanes(rows_of):
-        count = rows_of.shape[0]
-        split = rows_of.astype(F32).reshape(count, lane_blocks, 1, LANES).transpose(1, 0, 2, 3)
-        return jnp.broadcast_to(split, (lane_blocks, count, 8, LANES))
-
-    taps8 = by_lanes(conv_taps)
-    bias8 = by_lanes(conv_bias[None])[:, 0]
     gain = norm_gain.astype(F32)[None]
 
     tp_others = lax.axis_size("tp") - 1
@@ -446,6 +487,7 @@
 
     anywhere = pl.BlockSpec(memory_space=pl.ANY)
     stats_shape = (2, stat_rows, LANES)
+    taps_shape = (lane_blocks, K, 8, LANES)
     seq_blocks = tokens // rows
 
     def block_of(i):
@@ -455,22 +497,24 @@
     ahead_halo = pl.BlockSpec(
         (HALO, chans), lambda i: (jnp.maximum(block_of(i) * (rows // HALO) - 1, 0), 0)
     )
-    conv, swish_grad, sums, halo = pl.pallas_call(
+    conv, swish_grad, sums, halo, taps8 = pl.pallas_call(
         functools.partial(forward_kernel, seqs, seq_blocks),
         grid=(blocks,),
         in_specs=[
             tile, tile, ahead_halo, ahead_halo, anywhere, anywhere,
-            whole(taps8.shape),
-            whole(bias8.shape),
+            whole(conv_taps.shape),
+            whole((1, chans)),
             pl.BlockSpec((rows, width), lambda i: (block_of(i), 0)),
             whole(out_weight.shape),
         ],
-        out_specs=[tile, tile, whole(stats_shape), whole((seqs, HALO, chans))],
+        out_specs=[tile, tile, whole(stats_shape), whole((seqs, HALO, chans)),
+                   whole(taps_shape)],
         out_shape=[
             jax.ShapeDtypeStruct((positions, chans), F32),
             jax.ShapeDtypeStruct((positions, chans), F32),
             jax.ShapeDtypeStruct(stats_shape, F32),
             jax.ShapeDtypeStruct((seqs, HALO, chans), F32),
+            jax.ShapeDtypeStruct(taps_shape, F32),
         ],
         scratch_shapes=[
             pltpu.VMEM((lane_blocks, rows + HALO, LANES), F32),
@@ -481,7 +525,8 @@
         ],
         compiler_params=params(0),
         name="forward",
-    )(values, gates, values, gates, values_in, gates_in, taps8, bias8, cot, out_weight)
+    )(values, gates, values, gates, values_in, gates_in, conv_taps,
+      conv_bias[None], cot, out_weight)
 
     ahead = pl.BlockSpec((rows, chans), lambda i: (jnp.minimum(i, blocks - 1), 0))
     normed_grad, back, gain_local, weight_local, stats = pl.pallas_call(
@@ -522,6 +567,7 @@
 
     small_rows = -(-(K + 2) // 8) * 8
     weight_rows = chans // sp_devices
+    groups = sp_devices // PAIR if sp_devices % PAIR == 0 else sp_devices
     padded_shape = (seqs * lane_blocks, tokens + HALO, LANES)
     values_grad, gates_grad, small, weight_grad = pl.pallas_call(
         functools.partial(backward_kernel, total_chans, seqs),
@@ -545,15 +591,18 @@
             pltpu.VMEM((tp_others, *stats_shape), F32),
             pltpu.VMEM((small_rows, chans), F32),
             pltpu.VMEM((sp_others, small_rows, chans), F32),
-            pltpu.VMEM((weight_rows, width), BF16),
-            pltpu.VMEM((sp_others, weight_rows, width), BF16),
+            pltpu.VMEM((groups, weight_rows, width), BF16),
+            pltpu.VMEM((groups, weight_rows, width), BF16),
+            pltpu.VMEM((max(groups - 1, 1), weight_rows, width), BF16),
             dma(seqs, 4),
             dma(seqs, 2),
-            pltpu.SemaphoreType.DMA,
+            dma(groups),
+            dma(groups),
+            dma(groups),
             dma(tp_others),
             dma(tp_others),
-            dma(sp_others),
-            dma(sp_others),
+            dma(max(groups - 1, 1)),
+            dma(max(groups - 1, 1)),
             pltpu.SemaphoreType.DMA,
             pltpu.SemaphoreType.DMA,
             dma(sp_others),

time: 135 us -> 122 us (0.904)
  Pallas kernels: 122 us -> 111 us
    pallas_call x1, Pallas kernels: 59.4 us -> 48.2 us  [on_device(): pl.pallas_call(functools.partial(backward_kernel, total_chans, seqs), in_...]
where the time goes in v3:
time: 122 us
  Pallas kernels  111 us (91%)
  local copies, waits for them, and re-layouts  9.27 us (8%)
  other arithmetic  1.22 us (1%)
    pallas_call x1, Pallas kernels, on_device(): pl.pallas_call(functools.partial(backward_kernel, total_chans, seqs), in_...  48.2 us
    pallas_call x1, Pallas kernels, on_device(): pl.pallas_call(functools.partial(forward_kernel, seqs, seq_blocks), grid=...  33.8 us
    pallas_call x1, Pallas kernels, on_device(): pl.pallas_call(functools.partial(middle_kernel, blocks, total_chans), gri...  28.6 us
    unnamed x7, local copies, waits for them, and re-layouts  5.39 us

profile of v3, /device:TPU:0, one launch (start us, length us, event | category | flops | bytes accessed | tf_op | source)
XLA Modules:
  0.0 121.8 jit_solution(7734511177322597129)
XLA Ops:
  0.6 1.2 %broadcast_in_dim.8.bias_ref = bf16[1,256]{1,0:T(2,128)(2,1)} reshape(bf16[256]{0:T(256)(128)(2,1)} %param.10) | data formatting | bytes 1024 | tf_op jit(solution)/shard_map/broadcast_in_dim | solution.py:529
  1.9 1.2 %broadcast_in_dim.11 = f32[256]{0:T(256)} convert(bf16[256]{0:T(256)(128)(2,1)} %param.11) | non-fusion elementwise | flops 256 | bytes 1536 | tf_op jit(solution)/shard_map/broadcast_in_dim | solution.py:473
  3.1 33.8 %forward.1 = (f32[4096,256]{1,0:T(8,128)}, f32[4096,256]{1,0:T(8,128)}, f32[2,32,128]{2,1,0:T(8,128)}, f32[4,32,256]{2,1,0:T(8,128)}, f32[2,31,8,128]{3,2,1,0:T(8,128)}) custom-call(bf16[4096,256]{1,0:T(8,128)(2,1)} %bitcast.11, bf16[4096,256]{1,0:T(8,128)(2,1)} %bitcast.14, bf16[4096,256]{1,0:T(8,128)(2,1)} %bitcast.12, bf16[4096,256]{1,0:T(8,128)(2,1)} %bitcast.15, ...), custom_call_target="tpu_custom_call" | custom-call | tf_op jit(solution)/shard_map/forward/pallas_call | solution.py:500
  36.9 28.6 %middle.1 = (f32[4096,256]{1,0:T(8,128)}, f32[2,32,128]{2,1,0:T(8,128)}, f32[8,256]{1,0:T(8,128)}, bf16[256,4096]{1,0:T(8,128)(2,1)}, f32[2,32,128]{2,1,0:T(8,128)}) custom-call(f32[4096,256]{1,0:T(8,128)} %get-tuple-element.20.conv_ref.conv_hbm, f32[4096,256]{1,0:T(8,128)} %get-tuple-element.21.grad_ref, ...), custom_call_target="tpu_custom_call" | custom-call | tf_op jit(solution)/shard_map/middle/pallas_call | solution.py:532
  65.5 48.2 %backward.1 = (bf16[4096,256]{1,0:T(8,128)(2,1)}, bf16[4096,256]{1,0:T(8,128)(2,1)}, f32[40,256]{1,0:T(8,128)}, f32[32,4096]{1,0:T(8,128)}) custom-call(bf16[4096,256]{1,0:T(8,128)(2,1)} %bitcast.13, bf16[4096,256]{1,0:T(8,128)(2,1)} %bitcast.16, f32[4096,256]{1,0:T(8,128)} %get-tuple-element.20.conv_ref.conv_hbm, ...), custom_call_target="tpu_custom_call" | custom-call | tf_op jit(solution)/shard_map/backward/pallas_call | solution.py:572
  113.7 1.3 %fusion = (f32[1,256]{1,0:T(1,128)}, f32[1,256]{1,0:T(1,128)}) fusion(f32[40,256]{1,0:T(8,128)} %get-tuple-element.32), kind=kLoop, calls=%fused_computation | loop fusion | bytes 4096 | tf_op jit(solution)/shard_map/slice | solution.py:625
  115.0 1.4 %slice.9 = f32[31,256]{1,0:T(8,128)} slice(f32[40,256]{1,0:T(8,128)} %get-tuple-element.32), slice={[0:31], [0:256]} | slice | bytes 63488 | tf_op jit(solution)/shard_map/slice | solution.py:623
  116.4 0.0 copy-start
  116.4 3.2 %copy.16 = bf16[4,1024,256]{2,1,0:T(8,128)(2,1)} copy(bf16[4,1024,256]{2,1,0:T(8,128)(2,1)} %bitcast.18) | data formatting | bytes 4194304
  119.6 0.0 copy-done
  119.6 0.0 copy-start.1
  119.6 1.3 %copy.17 = bf16[4,1024,256]{2,1,0:T(8,128)(2,1)} copy(bf16[4,1024,256]{2,1,0:T(8,128)(2,1)S(1)} %bitcast.17) | data formatting | bytes 4194304
  120.9 0.1 copy-done.1
  121.0 0.8 copy.18
Async XLA Ops:
  116.4 3.2 %copy-start = (bf16[4096,256]{1,0:T(8,128)(2,1)S(1)}, bf16[4096,256]{1,0:T(8,128)(2,1)}, u32[]{:S(2)}) copy-start(bf16[4096,256]{1,0:T(8,128)(2,1)} %get-tuple-element.31) | copy-start | bytes 6291460
  119.6 1.4 %copy-start.1 = (f32[32,4096]{1,0:T(8,128)S(1)}, f32[32,4096]{1,0:T(8,128)}, u32[]{:S(2)}) copy-start(f32[32,4096]{1,0:T(8,128)} %get-tuple-element.47) | copy-start | bytes 1572868
